TPU v7x, 32 devices: a whole 2x2x4 slice. The times are simulated.
32 devices in a mesh: sp: 8 (over z, y), tp: 4 (over x, core).
Axes of the slice: x: 2, y: 2, z: 4, core: 2. Of those that a mesh axis runs over, the one named last changes fastest.
Arguments:
- tokens: bfloat16 [2048, 2048], P('sp'), may hold values from -72 to 72
- query_weight: bfloat16 [3, 2048, 1024], P(None, None, 'tp'), may hold values from -0.125 to 0.125
- key_weight: bfloat16 [3, 2048, 1024], P(None, None, 'tp'), may hold values from -0.125 to 0.125
- value_weight: bfloat16 [3, 2048, 1024], P(None, None, 'tp'), may hold values from -0.125 to 0.125
- out_weight: bfloat16 [1024, 2048], P(None, 'tp'), may hold values from -2 to 2
Outputs:
- mixed: bfloat16 [2048, 2048], P('sp', 'tp')
All inputs are finite; a program needn't handle non-finite values.
Results may differ from a plain program's by a relative error of at most 0.012.
Values may be sent and summed in bfloat16 or wider, within the bound.
A program may use at most 64 MiB of HBM per device.

v0:
```python
import math

import jax
import jax.numpy as jnp
from jax import lax
from jax.sharding import PartitionSpec as P

HEAD_DIM = 64
SIDE_STEPS = 64
MIDDLE_DILATION = 4
FAR_DILATION = 16


def shifted(block, axis, distance):
    devices = range(lax.axis_size(axis))
    route = [(i - distance, i) for i in devices if i - distance in devices]
    return lax.ppermute(block, axis, route)


def with_halo(block, sides, width):
    for axis, dim in sides:
        count = lax.axis_size(axis)
        forward = [(i, i + 1) for i in range(count - 1)]
        backward = [(target, source) for source, target in forward]
        low = lax.ppermute(
            lax.slice_in_dim(block, block.shape[dim] - width, None, axis=dim), axis, forward
        )
        high = lax.ppermute(lax.slice_in_dim(block, 0, width, axis=dim), axis, backward)
        block = jnp.concatenate([low, block, high], axis=dim)
    return block


def rotate(projected, offset_pos):
    length, columns = projected.shape
    heads = columns // HEAD_DIM
    half = HEAD_DIM // 2
    positions = (offset_pos + jnp.arange(length)).astype(jnp.float32)
    inverse = 1.0 / 10000.0 ** (jnp.arange(half, dtype=jnp.float32) * 2.0 / HEAD_DIM)
    angles = positions[:, None] * inverse[None, :]
    angles = jnp.concatenate([angles, angles], axis=-1)
    cosine_table = jnp.cos(angles)[:, None, :]
    sine = jnp.sin(angles)[:, None, :]
    shaped = projected.reshape(length, heads, HEAD_DIM)
    turned = jnp.concatenate([-shaped[..., half:], shaped[..., :half]], axis=-1)
    return (shaped * cosine_table + turned * sine).reshape(length, columns)


def banded(queries, key_ext, value_ext, dilation, offset_pos, seq_len):
    length, columns = queries.shape
    heads = columns // HEAD_DIM
    class_len = length // dilation
    block_len = math.gcd(SIDE_STEPS, class_len)
    blocks = class_len // block_len
    extra = 2 * SIDE_STEPS // block_len
    query_blocks = queries.reshape(blocks, block_len, dilation, heads, HEAD_DIM)
    key_blocks = key_ext.reshape(blocks + extra, block_len, dilation, heads, HEAD_DIM)
    value_blocks = value_ext.reshape(blocks + extra, block_len, dilation, heads, HEAD_DIM)
    key_win = jnp.concatenate(
        [key_blocks[shift_idx : shift_idx + blocks] for shift_idx in range(extra + 1)], axis=1
    )
    value_win = jnp.concatenate(
        [value_blocks[shift_idx : shift_idx + blocks] for shift_idx in range(extra + 1)], axis=1
    )
    scores = jnp.einsum(
        "bqrhe,bkrhe->brhqk", query_blocks, key_win, preferred_element_type=jnp.float32
    )
    scores = scores * HEAD_DIM ** (-0.5)
    width_keys = key_win.shape[1]
    relative = jnp.arange(width_keys)[None, :] - jnp.arange(block_len)[:, None]
    within = (relative >= 0) & (relative <= 2 * SIDE_STEPS)
    key_rows = jnp.arange(blocks)[:, None] * block_len + jnp.arange(width_keys)[None, :]
    spots = (
        offset_pos
        - SIDE_STEPS * dilation
        + dilation * key_rows[:, :, None]
        + jnp.arange(dilation)[None, None, :]
    )
    inside = (spots >= 0) & (spots < seq_len)
    allowed = within[None, None, None] & jnp.transpose(inside, (0, 2, 1))[:, :, None, None, :]
    scores = jnp.where(allowed, scores, -1e30)
    row_max = jnp.max(scores, axis=-1, keepdims=True)
    expo = jnp.exp(scores - row_max)
    denom = jnp.sum(expo, axis=-1)
    probs = expo.astype(jnp.bfloat16)
    summed = jnp.einsum("brhqk,bkrhe->bqrhe", probs, value_win, preferred_element_type=jnp.float32)
    group_out = summed / jnp.transpose(denom, (0, 3, 1, 2))[..., None]
    log_sum = row_max[..., 0] + jnp.log(denom)
    log_sum = jnp.transpose(log_sum, (0, 3, 1, 2)).reshape(length, heads)
    return (group_out.reshape(length, columns), log_sum)


def collect(own_block, needed, direction):
    collected = own_block[None]
    while collected.shape[0] < needed + 1:
        stride = collected.shape[0]
        to_send = min(stride, needed + 1 - stride)
        arrived = shifted(collected[:to_send], "sp", direction * stride)
        collected = jnp.concatenate([collected, arrived], axis=0)
    return collected[1:]


def per_device(tokens, query_weight, key_weight, value_weight, out_weight):
    length = tokens.shape[0]
    offset_pos = lax.axis_index("sp") * length
    seq_len = lax.axis_size("sp") * length
    group_dilations = (1, MIDDLE_DILATION, FAR_DILATION)
    query_list = []
    pairs = []
    for group_idx in range(3):
        queries = rotate(
            jnp.dot(tokens, query_weight[group_idx], preferred_element_type=jnp.float32), offset_pos
        )
        keys_here = rotate(
            jnp.dot(tokens, key_weight[group_idx], preferred_element_type=jnp.float32), offset_pos
        )
        values_here = jnp.dot(tokens, value_weight[group_idx], preferred_element_type=jnp.float32)
        query_list.append(queries.astype(jnp.bfloat16))
        pairs.append(
            jnp.stack([keys_here.astype(jnp.bfloat16), values_here.astype(jnp.bfloat16)], axis=0)
        )
    middle_span_length = SIDE_STEPS * MIDDLE_DILATION
    first_ext = with_halo(pairs[0], (("sp", 1),), SIDE_STEPS)
    middle_ext = with_halo(pairs[1], (("sp", 1),), middle_span_length)
    far_span_length = SIDE_STEPS * FAR_DILATION
    needed = -(-far_span_length // length)
    lower_blocks = collect(pairs[2], needed, 1)
    upper_blocks = collect(pairs[2], needed, -1)
    columns = pairs[2].shape[2]
    lower_flat = jnp.moveaxis(lower_blocks[::-1], 0, 1).reshape(2, needed * length, columns)
    upper_flat = jnp.moveaxis(upper_blocks, 0, 1).reshape(2, needed * length, columns)
    far_full = jnp.concatenate([lower_flat, pairs[2], upper_flat], axis=1)
    extended = (first_ext, middle_ext, far_full)
    outputs = []
    log_sums = []
    for group_idx in range(3):
        group_out, log_sum = banded(
            query_list[group_idx],
            extended[group_idx][0],
            extended[group_idx][1],
            group_dilations[group_idx],
            offset_pos,
            seq_len,
        )
        outputs.append(group_out)
        log_sums.append(log_sum)
    merge_w = jax.nn.softmax(jnp.stack(log_sums, axis=0), axis=0)
    heads = columns // HEAD_DIM
    stacked = jnp.stack(outputs, axis=0).reshape(3, length, heads, HEAD_DIM)
    merged = (
        jnp.sum(merge_w[..., None] * stacked, axis=0).reshape(length, columns).astype(jnp.bfloat16)
    )
    mixed = jnp.dot(
        lax.all_gather(merged, "tp", axis=1, tiled=True),
        out_weight,
        preferred_element_type=jnp.float32,
    )
    return mixed.astype(jnp.bfloat16)


def solution(mesh):
    placed = (
        P("sp", None),
        P(None, None, "tp"),
        P(None, None, "tp"),
        P(None, None, "tp"),
        P(None, "tp"),
    )
    return jax.shard_map(
        per_device, mesh=mesh, in_specs=placed, out_specs=P("sp", "tp"), check_vma=False
    )
```

profile of v0, /device:TPU:9, one launch (start us, length us, event | category | flops | bytes accessed | tf_op | source)
XLA Modules:
  0.0 185.7 jit_solution(4766220064842487170)
XLA Ops:
  0.0 3.1 %slice_bitcast_fusion.4 = (bf16[256,2048]{0,1:T(8,128)(2,1)S(1)}, bf16[256,2048]{0,1:T(8,128)(2,1)}, bf16[256,2048]{0,1:T(8,128)(2,1)S(1)}) fusion(bf16[3,2048,256]{2,1,0:T(8,128)(2,1)} %param.7), kind=kLoop, calls=%fused_computation.45 | loop fusion | bytes 6291456 | tf_op jit(solution)/shard_map/dot_general | solution.py:114
  3.1 2.3 %copy.111 = bf16[256,2048]{1,0:T(8,128)(2,1)} copy(bf16[256,2048]{0,1:T(8,128)(2,1)} %get-tuple-element.9) | data formatting | bytes 2097152 | tf_op jit(solution)/shard_map/dot_general | solution.py:114
  14.2 4.9 %collective-permute-start.6 = (bf16[1,2,256,256]{3,2,1,0:T(8,128)(2,1)}, bf16[1,2,256,256]{3,2,1,0:T(8,128)(2,1)}, u32[]{:S(2)}, u32[]{:S(2)}) collective-permute-start(bf16[1,2,256,256]{3,2,1,0:T(8,128)(2,1)} %maximum_bitcast_fusion.9), channel_id=1, source_target_pairs={{0,16},{4,20},{8,24},{12,28},{1,17},{5,21},{9,25},{13,29},{2,18},{... | collective-permute-start | bytes 786440 | tf_op jit(solution)/shard_map/ppermute | solution.py:17
  19.1 3.0 %collective-permute-start.7 = (bf16[1,2,256,256]{3,2,1,0:T(8,128)(2,1)}, bf16[1,2,256,256]{3,2,1,0:T(8,128)(2,1)}, u32[]{:S(2)}, u32[]{:S(2)}) collective-permute-start(bf16[1,2,256,256]{3,2,1,0:T(8,128)(2,1)} %maximum_bitcast_fusion.9), channel_id=1, source_target_pairs={{4,0},{8,4},{12,8},{16,12},{20,16},{24,20},{28,24},{5,1},{9,5},{13... | collective-permute-start | bytes 786440 | tf_op jit(solution)/shard_map/ppermute | solution.py:17
  22.1 2.3 %collective-permute-start.4 = (bf16[1,2,256,256]{3,2,1,0:T(8,128)(2,1)}, bf16[1,2,256,256]{3,2,1,0:T(8,128)(2,1)}, u32[]{:S(2)}, u32[]{:S(2)}) collective-permute-start(bf16[1,2,256,256]{3,2,1,0:T(8,128)(2,1)} %maximum_bitcast_fusion.9), channel_id=1, source_target_pairs={{0,4},{4,8},{8,12},{12,16},{16,20},{20,24},{24,28},{1,5},{5,9},{9,... | collective-permute-start | bytes 786440 | tf_op jit(solution)/shard_map/ppermute | solution.py:17
  27.7 2.3 %copy.91 = bf16[256,2048]{1,0:T(8,128)(2,1)} copy(bf16[256,2048]{0,1:T(8,128)(2,1)} %get-tuple-element.5) | data formatting | bytes 2097152 | tf_op jit(solution)/shard_map/dot_general | solution.py:111
  33.1 2.3 %copy.99 = bf16[256,2048]{1,0:T(8,128)(2,1)} copy(bf16[256,2048]{0,1:T(8,128)(2,1)} %get-tuple-element.7) | data formatting | bytes 2097152 | tf_op jit(solution)/shard_map/dot_general | solution.py:111
  35.4 2.4 %fusion.24 = f32[256,4,64]{0,2,1:T(8,128)} fusion(bf16[4,64,2048]{2,1,0:T(8,128)(2,1)} %bitcast.222, bf16[256,2048]{1,0:T(8,128)(2,1)S(1)} %copy-done), kind=kOutput, calls=%fused_computation.28 | convolution fusion | flops 268435456 | bytes 2359296 | tf_op jit(solution)/shard_map/dot_general | solution.py:111
  39.2 2.5 %fusion.26 = f32[256,4,64]{0,2,1:T(8,128)} fusion(bf16[4,64,2048]{2,1,0:T(8,128)(2,1)} %bitcast.223, bf16[256,2048]{1,0:T(8,128)(2,1)S(1)} %copy-done), kind=kOutput, calls=%fused_computation.30 | convolution fusion | flops 268435456 | bytes 2359296 | tf_op jit(solution)/shard_map/dot_general | solution.py:114
  43.1 2.4 %fusion.20 = f32[256,4,64]{0,2,1:T(8,128)} fusion(bf16[4,64,2048]{2,1,0:T(8,128)(2,1)} %bitcast.224, bf16[256,2048]{1,0:T(8,128)(2,1)S(1)} %copy-done), kind=kOutput, calls=%fused_computation.24 | convolution fusion | flops 268435456 | bytes 2359296 | tf_op jit(solution)/shard_map/dot_general | solution.py:111
  49.7 4.0 %collective-permute-start = (bf16[2,64,256]{2,1,0:T(8,128)(2,1)}, bf16[2,64,256]{2,1,0:T(8,128)(2,1)}, u32[]{:S(2)}, u32[]{:S(2)}) collective-permute-start(bf16[2,64,256]{2,1,0:T(8,128)(2,1)} %get-tuple-element.35), channel_id=1, source_target_pairs={{0,4},{4,8},{8,12},{12,16},{16,20},{20,24},{24,28},{1,5},{5,9},{9,... | collective-permute-start | bytes 196616 | tf_op jit(solution)/shard_map/ppermute | solution.py:25
  53.8 2.1 %collective-permute-start.1 = (bf16[2,64,256]{2,1,0:T(8,128)(2,1)}, bf16[2,64,256]{2,1,0:T(8,128)(2,1)}, u32[]{:S(2)}, u32[]{:S(2)}) collective-permute-start(bf16[2,64,256]{2,1,0:T(8,128)(2,1)} %get-tuple-element.36), channel_id=1, source_target_pairs={{4,0},{8,4},{12,8},{16,12},{20,16},{24,20},{28,24},{5,1},{9,5},{13... | collective-permute-start | bytes 196616 | tf_op jit(solution)/shard_map/ppermute | solution.py:28
  71.9 3.8 %collective-permute-start.3 = (bf16[2,256,256]{2,1,0:T(8,128)(2,1)}, bf16[2,256,256]{2,1,0:T(8,128)(2,1)}, u32[]{:S(2)}, u32[]{:S(2)}) collective-permute-start(bf16[2,256,256]{2,1,0:T(8,128)(2,1)} %pad_maximum_fusion.3), channel_id=1, source_target_pairs={{4,0},{8,4},{12,8},{16,12},{20,16},{24,20},{28,24},{5,1},{9,5},{13... | collective-permute-start | bytes 786440 | tf_op jit(solution)/shard_map/ppermute | solution.py:28
  86.4 4.7 %collective-permute-start.5 = (bf16[2,2,256,256]{3,2,1,0:T(8,128)(2,1)}, bf16[2,2,256,256]{3,2,1,0:T(8,128)(2,1)}, u32[]{:S(2)}, u32[]{:S(2)}) collective-permute-start(bf16[2,2,256,256]{3,2,1,0:T(8,128)(2,1)} %get-tuple-element.50), channel_id=1, source_target_pairs={{0,8},{4,12},{8,16},{12,20},{16,24},{20,28},{1,9},{5,13},{9,17},{1... | collective-permute-start | bytes 1572872 | tf_op jit(solution)/shard_map/ppermute | solution.py:17
  103.4 2.4 %fusion.37 = f32[1,64,4,4,64]{1,4,3,2,0:T(8,128)} fusion(f32[4,4,64,192]{3,2,1,0:T(8,128)S(1)} %get-tuple-element.65, bf16[1,64,4,4,64]{1,4,3,2,0:T(8,128)(2,1)} %copy.136, bf16[1,64,4,4,64]{1,4,3,2,0:T(8,128)(2,1)} %copy.135, bf16[1,64,4,4,64]{1,4,3,2,0:T(8,128)(2,1)} %copy.134, f32[4,4,64]{2,1,0:T(4,128)S(1)} %get-tuple-element.64, f32[64,4,4]{0,2,1:T(4,128)} %bitcast.233), kind=kOutput, calls=%fused_computation.49 | convolution fusion | flops 26804224 | bytes 1449984 | tf_op jit(solution)/shard_map/brhqk,bkrhe->bqrhe/dot_general | solution.py:85
  110.2 3.2 %collective-permute-done.8 = bf16[2,2,256,256]{3,2,1,0:T(8,128)(2,1)} collective-permute-done((bf16[2,2,256,256]{3,2,1,0:T(8,128)(2,1)S(1)}, bf16[2,2,256,256]{3,2,1,0:T(8,128)(2,1)}, u32[]{:S(2)}, u32[]{:S(2)}) %collective-permute-start.8) | collective-permute-done | bytes 524320 | tf_op jit(solution)/shard_map/ppermute | solution.py:17
  128.3 9.6 %concatenate.99 = bf16[1,144,16,4,64]{1,4,3,2,0:T(8,128)(2,1)S(1)} concatenate(bf16[1,16,16,4,64]{1,4,3,2,0:T(8,128)(2,1)} %copy.116, bf16[1,16,16,4,64]{1,4,3,2,0:T(8,128)(2,1)} %copy.117, bf16[1,16,16,4,64]{1,4,3,2,0:T(8,128)(2,1)} %copy.118, bf16[1,16,16,4,64]{1,4,3,2,0:T(8,128)(2,1)} %copy.119, bf16[1,16,16,4,64]{1,4,3,2,0:T(8,128)(2,1)S(1)} %copy.120, ...), dimensions={1} | concatenate | bytes 2359296 | tf_op jit(solution)/shard_map/concatenate | solution.py:58
  147.8 2.5 %copy.143 = bf16[1,16,16,4,64]{1,4,3,2,0:T(8,128)(2,1)} copy(bf16[1,16,16,4,64]{4,3,2,1,0:T(4,128)(2,1)} %slice.368) | data formatting | bytes 262144 | tf_op jit(solution)/shard_map/slice | solution.py:62
  152.1 2.3 %copy.144 = bf16[1,16,16,4,64]{1,4,3,2,0:T(8,128)(2,1)} copy(bf16[1,16,16,4,64]{4,3,2,1,0:T(4,128)(2,1)} %slice.370) | data formatting | bytes 262144 | tf_op jit(solution)/shard_map/slice | solution.py:62
  156.2 2.4 %copy.145 = bf16[1,16,16,4,64]{1,4,3,2,0:T(8,128)(2,1)} copy(bf16[1,16,16,4,64]{4,3,2,1,0:T(4,128)(2,1)} %slice.372) | data formatting | bytes 262144 | tf_op jit(solution)/shard_map/slice | solution.py:62
  159.5 2.4 %copy.146 = bf16[1,16,16,4,64]{1,4,3,2,0:T(8,128)(2,1)} copy(bf16[1,16,16,4,64]{4,3,2,1,0:T(4,128)(2,1)} %slice.374) | data formatting | bytes 262144 | tf_op jit(solution)/shard_map/slice | solution.py:62
  161.9 10.3 %concatenate.102 = bf16[1,144,16,4,64]{1,4,3,2,0:T(8,128)(2,1)} concatenate(bf16[1,16,16,4,64]{1,4,3,2,0:T(8,128)(2,1)S(1)} %copy.138, bf16[1,16,16,4,64]{1,4,3,2,0:T(8,128)(2,1)} %copy.139, bf16[1,16,16,4,64]{1,4,3,2,0:T(8,128)(2,1)} %copy.140, bf16[1,16,16,4,64]{1,4,3,2,0:T(8,128)(2,1)} %copy.141, bf16[1,16,16,4,64]{1,4,3,2,0:T(8,128)(2,1)S(1)} %copy-done.3, ...), dimensions={1} | concatenate | bytes 2359296 | tf_op jit(solution)/shard_map/concatenate | solution.py:61
  172.2 2.4 %fusion.33 = f32[1,16,16,4,64]{4,1,3,2,0:T(8,128)S(1)} fusion(bf16[1,144,16,4,64]{1,4,3,2,0:T(8,128)(2,1)} %concatenate.102, f32[16,4,16,144]{3,2,1,0:T(8,128)S(1)} %get-tuple-element.63, f32[16,4,16]{2,1,0:T(4,128)S(1)} %copy-done.24, f32[16,16,4]{0,2,1:T(4,128)S(1)} %bitcast.232), kind=kOutput, calls=%fused_computation.47 | convolution fusion | flops 19234816 | bytes 2039808 | tf_op jit(solution)/shard_map/brhqk,bkrhe->bqrhe/dot_general | solution.py:85
  175.3 9.2 %all_gather.3 = bf16[256,1024]{0,1:T(8,128)(2,1)S(1)} all-gather(bf16[256,256]{0,1:T(8,128)(2,1)S(1)} %bitcast.228), channel_id=1, replica_groups=mesh['sp'=8,'tp'=4] {'tp'}, dimensions={1}, use_global_device_ids=true | all-gather | bytes 655360 | tf_op jit(solution)/shard_map/all_gather | solution.py:153
  (216 shorter events, 96.0 us)
Async XLA Ops:
  0.0 5.4 %copy-start = (bf16[256,2048]{1,0:T(8,128)(2,1)S(1)}, bf16[256,2048]{1,0:T(8,128)(2,1)}, u32[]{:S(2)}) copy-start(bf16[256,2048]{1,0:T(8,128)(2,1)} %param.5) | copy-start | bytes 3145732
  7.1 15.0 %copy-start.16 = (bf16[256,256]{1,0:T(8,128)(2,1)}, bf16[256,256]{1,0:T(8,128)(2,1)S(1)}, u32[]{:S(2)}) copy-start(bf16[256,256]{1,0:T(8,128)(2,1)S(1)} %convolution_convert_fusion.1) | copy-start | bytes 393220
  12.4 13.7 %copy-start.4 = (bf16[3,2048,256]{2,1,0:T(8,128)(2,1)S(1)}, bf16[3,2048,256]{2,1,0:T(8,128)(2,1)}, u32[]{:S(2)}) copy-start(bf16[3,2048,256]{2,1,0:T(8,128)(2,1)} %param.6) | copy-start | bytes 9437188
  14.2 93.8 %collective-permute-start.6 = (bf16[1,2,256,256]{3,2,1,0:T(8,128)(2,1)}, bf16[1,2,256,256]{3,2,1,0:T(8,128)(2,1)}, u32[]{:S(2)}, u32[]{:S(2)}) collective-permute-start(bf16[1,2,256,256]{3,2,1,0:T(8,128)(2,1)} %maximum_bitcast_fusion.9), channel_id=1, source_target_pairs={{0,16},{4,20},{8,24},{12,28},{1,17},{5,21},{9,25},{13,29},{2,18},{... | collective-permute-start | bytes 786440 | tf_op jit(solution)/shard_map/ppermute | solution.py:17
  19.1 63.4 %collective-permute-start.7 = (bf16[1,2,256,256]{3,2,1,0:T(8,128)(2,1)}, bf16[1,2,256,256]{3,2,1,0:T(8,128)(2,1)}, u32[]{:S(2)}, u32[]{:S(2)}) collective-permute-start(bf16[1,2,256,256]{3,2,1,0:T(8,128)(2,1)} %maximum_bitcast_fusion.9), channel_id=1, source_target_pairs={{4,0},{8,4},{12,8},{16,12},{20,16},{24,20},{28,24},{5,1},{9,5},{13... | collective-permute-start | bytes 786440 | tf_op jit(solution)/shard_map/ppermute | solution.py:17
  22.1 62.3 %collective-permute-start.4 = (bf16[1,2,256,256]{3,2,1,0:T(8,128)(2,1)}, bf16[1,2,256,256]{3,2,1,0:T(8,128)(2,1)}, u32[]{:S(2)}, u32[]{:S(2)}) collective-permute-start(bf16[1,2,256,256]{3,2,1,0:T(8,128)(2,1)} %maximum_bitcast_fusion.9), channel_id=1, source_target_pairs={{0,4},{4,8},{8,12},{12,16},{16,20},{20,24},{24,28},{1,5},{5,9},{9,... | collective-permute-start | bytes 786440 | tf_op jit(solution)/shard_map/ppermute | solution.py:17
  46.7 9.2 %copy-start.17 = (bf16[256,256]{1,0:T(8,128)(2,1)S(1)}, bf16[256,256]{1,0:T(8,128)(2,1)}, u32[]{:S(2)}) copy-start(bf16[256,256]{1,0:T(8,128)(2,1)} %copy-done.16) | copy-start | bytes 393220
  49.7 20.8 %collective-permute-start = (bf16[2,64,256]{2,1,0:T(8,128)(2,1)}, bf16[2,64,256]{2,1,0:T(8,128)(2,1)}, u32[]{:S(2)}, u32[]{:S(2)}) collective-permute-start(bf16[2,64,256]{2,1,0:T(8,128)(2,1)} %get-tuple-element.35), channel_id=1, source_target_pairs={{0,4},{4,8},{8,12},{12,16},{16,20},{20,24},{24,28},{1,5},{5,9},{9,... | collective-permute-start | bytes 196616 | tf_op jit(solution)/shard_map/ppermute | solution.py:25
  53.8 18.2 %collective-permute-start.1 = (bf16[2,64,256]{2,1,0:T(8,128)(2,1)}, bf16[2,64,256]{2,1,0:T(8,128)(2,1)}, u32[]{:S(2)}, u32[]{:S(2)}) collective-permute-start(bf16[2,64,256]{2,1,0:T(8,128)(2,1)} %get-tuple-element.36), channel_id=1, source_target_pairs={{4,0},{8,4},{12,8},{16,12},{20,16},{24,20},{28,24},{5,1},{9,5},{13... | collective-permute-start | bytes 196616 | tf_op jit(solution)/shard_map/ppermute | solution.py:28
  58.5 5.5 %copy-start.19 = (bf16[256,4,64]{0,2,1:T(8,128)(2,1)S(1)}, bf16[256,4,64]{0,2,1:T(8,128)(2,1)}, u32[]{:S(2)}) copy-start(bf16[256,4,64]{0,2,1:T(8,128)(2,1)} %get-tuple-element.55) | copy-start | bytes 393220
  59.3 6.7 %copy-start.18 = (bf16[256,4,64]{0,2,1:T(8,128)(2,1)S(1)}, bf16[256,4,64]{0,2,1:T(8,128)(2,1)}, u32[]{:S(2)}) copy-start(bf16[256,4,64]{0,2,1:T(8,128)(2,1)} %get-tuple-element.53) | copy-start | bytes 393220
  70.5 9.0 %copy-start.29 = (pred[4,64,192]{2,1,0:T(8,128)(4,1)S(1)}, pred[4,64,192]{2,1,0:T(8,128)(4,1)}, u32[]{:S(2)}) copy-start(pred[4,64,192]{2,1,0:T(8,128)(4,1)} %get-tuple-element.60) | copy-start | bytes 147460
  70.5 39.7 %collective-permute-start.9 = (bf16[1,2,256,256]{3,2,1,0:T(8,128)(2,1)}, bf16[1,2,256,256]{3,2,1,0:T(8,128)(2,1)}, u32[]{:S(2)}, u32[]{:S(2)}) collective-permute-start(bf16[1,2,256,256]{3,2,1,0:T(8,128)(2,1)} %maximum_bitcast_fusion.9), channel_id=1, source_target_pairs={{16,0},{20,4},{24,8},{28,12},{17,1},{21,5},{25,9},{29,13},{18,2},{... | collective-permute-start | bytes 786440 | tf_op jit(solution)/shard_map/ppermute | solution.py:17
  71.9 19.1 %collective-permute-start.3 = (bf16[2,256,256]{2,1,0:T(8,128)(2,1)}, bf16[2,256,256]{2,1,0:T(8,128)(2,1)}, u32[]{:S(2)}, u32[]{:S(2)}) collective-permute-start(bf16[2,256,256]{2,1,0:T(8,128)(2,1)} %pad_maximum_fusion.3), channel_id=1, source_target_pairs={{4,0},{8,4},{12,8},{16,12},{20,16},{24,20},{28,24},{5,1},{9,5},{13... | collective-permute-start | bytes 786440 | tf_op jit(solution)/shard_map/ppermute | solution.py:28
  82.5 12.5 %collective-permute-start.2 = (bf16[2,256,256]{2,1,0:T(8,128)(2,1)}, bf16[2,256,256]{2,1,0:T(8,128)(2,1)S(1)}, u32[]{:S(2)}, u32[]{:S(2)}) collective-permute-start(bf16[2,256,256]{2,1,0:T(8,128)(2,1)} %pad_maximum_fusion.3), channel_id=1, source_target_pairs={{0,4},{4,8},{8,12},{12,16},{16,20},{20,24},{24,28},{1,5},{5,9},{9,... | collective-permute-start | bytes 786440 | tf_op jit(solution)/shard_map/ppermute | solution.py:25
  86.4 21.5 %collective-permute-start.5 = (bf16[2,2,256,256]{3,2,1,0:T(8,128)(2,1)}, bf16[2,2,256,256]{3,2,1,0:T(8,128)(2,1)}, u32[]{:S(2)}, u32[]{:S(2)}) collective-permute-start(bf16[2,2,256,256]{3,2,1,0:T(8,128)(2,1)} %get-tuple-element.50), channel_id=1, source_target_pairs={{0,8},{4,12},{8,16},{12,20},{16,24},{20,28},{1,9},{5,13},{9,17},{1... | collective-permute-start | bytes 1572872 | tf_op jit(solution)/shard_map/ppermute | solution.py:17
  99.1 14.2 %collective-permute-start.8 = (bf16[2,2,256,256]{3,2,1,0:T(8,128)(2,1)S(1)}, bf16[2,2,256,256]{3,2,1,0:T(8,128)(2,1)}, u32[]{:S(2)}, u32[]{:S(2)}) collective-permute-start(bf16[2,2,256,256]{3,2,1,0:T(8,128)(2,1)S(1)} %get-tuple-element.49), channel_id=1, source_target_pairs={{8,0},{12,4},{16,8},{20,12},{24,16},{28,20},{9,1},{13,5},{17,9},{2... | collective-permute-start | bytes 1572872 | tf_op jit(solution)/shard_map/ppermute | solution.py:17
  141.6 5.3 %copy-start.15 = (bf16[1,256,256]{2,1,0:T(8,128)(2,1)S(1)}, bf16[1,256,256]{2,1,0:T(8,128)(2,1)}, u32[]{:S(2)}) copy-start(bf16[1,256,256]{2,1,0:T(8,128)(2,1)} %get-tuple-element.15) | copy-start | bytes 393220
  145.5 13.1 %copy-start.14 = (bf16[1,256,256]{2,1,0:T(8,128)(2,1)S(1)}, bf16[1,256,256]{2,1,0:T(8,128)(2,1)}, u32[]{:S(2)}) copy-start(bf16[1,256,256]{2,1,0:T(8,128)(2,1)} %get-tuple-element.12) | copy-start | bytes 393220
  147.8 14.0 %copy-start.3 = (bf16[1,16,16,4,64]{1,4,3,2,0:T(8,128)(2,1)S(1)}, bf16[1,16,16,4,64]{1,4,3,2,0:T(8,128)(2,1)}, u32[]{:S(2)}) copy-start(bf16[1,16,16,4,64]{1,4,3,2,0:T(8,128)(2,1)} %copy.142) | copy-start | bytes 393220
  161.9 10.3 %copy-start.24 = (f32[16,4,16]{2,1,0:T(4,128)S(1)}, f32[16,4,16]{2,1,0:T(4,128)}, u32[]{:S(2)}) copy-start(f32[16,4,16]{2,1,0:T(4,128)} %copy-done.23) | copy-start | bytes 12292
  161.9 10.3 %copy-start.28 = (f32[16,4,16]{2,1,0:T(4,128)S(1)}, f32[16,4,16]{2,1,0:T(4,128)}, u32[]{:S(2)}) copy-start(f32[16,4,16]{2,1,0:T(4,128)} %copy-done.27) | copy-start | bytes 12292
  172.2 13.4 %copy-start.1 = (bf16[256,2048]{1,0:T(8,128)(2,1)S(1)}, bf16[256,2048]{1,0:T(8,128)(2,1)}, u32[]{:S(2)}) copy-start(bf16[256,2048]{1,0:T(8,128)(2,1)} %param.5) | copy-start | bytes 3145732
  174.6 9.8 %copy-start.33 = (bf16[1024,512]{1,0:T(8,128)(2,1)S(1)}, bf16[1024,512]{1,0:T(8,128)(2,1)}, u32[]{:S(2)}) copy-start(bf16[1024,512]{1,0:T(8,128)(2,1)} %param.9) | copy-start | bytes 3145732
  (20 other events, 42.8 us)
where the time goes:
time: 189 us; the launch traced here: 186 us
  local copies, waits for them, and re-layouts  93.4 us (49%)
  starting transfers between devices  30.1 us (16%)
  matrix products  26.3 us (14%)
  other arithmetic  20.8 us (11%)
  blocking collectives  9.17 us (5%)
  waiting for transfers between devices  4.95 us (3%)
    slice x32, local copies, waits for them, and re-layouts, banded(): value_blocks[shift_idx:shift_idx + blocks]  29.6 us
    ppermute x6, starting transfers between devices, shifted(): return lax.ppermute(block, axis, route)  18.2 us
    slice x26, local copies, waits for them, and re-layouts, banded(): key_blocks[shift_idx:shift_idx + blocks]  17.3 us
    concatenate x1, local copies, waits for them, and re-layouts, banded(): jnp.concatenate([value_blocks[shift_idx:shift_idx + blocks] for shift_idx...  10.3 us
    concatenate x1, local copies, waits for them, and re-layouts, banded(): jnp.concatenate([key_blocks[shift_idx:shift_idx + blocks] for shift_idx i...  9.59 us
    all_gather x1, blocking collectives, per_device(): lax.all_gather(merged, 'tp', axis=1, tiled=True)  9.17 us
    dot_general x4, local copies, waits for them, and re-layouts, per_device(): jnp.dot(tokens, query_weight[group_idx], preferred_element_type=jnp.float32)  7.65 us
    dot_general x4, local copies, waits for them, and re-layouts, per_device(): jnp.dot(tokens, key_weight[group_idx], preferred_element_type=jnp.float32)  7.46 us
  transfers between devices with their start and end apart: 10, of which 2 were waited for; matrix products, arithmetic and copies ran while one was open for 34% of the time, Pallas kernels for 0%

commit v1 on v0

--- a/solution.py
+++ b/solution.py
@@ -1,14 +1,19 @@
+import functools
 import math
 
 import jax
+import numpy as np
 import jax.numpy as jnp
 from jax import lax
+from jax.experimental import pallas as pl
+from jax.experimental.pallas import tpu as pltpu
 from jax.sharding import PartitionSpec as P
 
 HEAD_DIM = 64
 SIDE_STEPS = 64
 MIDDLE_DILATION = 4
 FAR_DILATION = 16
+MESH = pl.DeviceIdType.MESH
 
 
 def shifted(block, axis, distance):
@@ -157,6 +162,434 @@
     return mixed.astype(jnp.bfloat16)
 
 
+def remote(src, dst, send_sem, recv_sem, axis, target):
+    return pltpu.make_async_remote_copy(
+        src_ref=src,
+        dst_ref=dst,
+        send_sem=send_sem,
+        recv_sem=recv_sem,
+        device_id={axis: target},
+        device_id_type=MESH,
+    )
+
+
+def head_mask(columns, head):
+    lane = lax.broadcasted_iota(jnp.int32, (1, columns), 1)
+    return (lane // HEAD_DIM == head).astype(jnp.float32)
+
+
+def attend(queries, keys, values, bias):
+    rows, columns = queries.shape
+    heads = columns // HEAD_DIM
+    masks = [head_mask(columns, head) for head in range(heads)]
+    stacked = jnp.concatenate([queries * mask.astype(jnp.bfloat16) for mask in masks], axis=0)
+    scores = lax.dot_general(
+        stacked, keys, (((1,), (1,)), ((), ())), preferred_element_type=jnp.float32
+    )
+    width = keys.shape[0]
+    scores = (scores.reshape(heads, rows, width) + bias[None]).reshape(heads * rows, width)
+    row_max = jnp.max(scores, axis=-1, keepdims=True)
+    expo = jnp.exp(scores - row_max)
+    denom = jnp.sum(expo, axis=-1, keepdims=True)
+    summed = jnp.dot(expo.astype(jnp.bfloat16), values, preferred_element_type=jnp.float32)
+    summed = summed / denom
+    lse = row_max + jnp.log(denom)
+    parts = [slice(head * rows, (head + 1) * rows) for head in range(heads)]
+    out = sum(summed[part] * mask for part, mask in zip(parts, masks))
+    return out, [lse[part] for part in parts]
+
+
+def packed_lse(lses):
+    heads = len(lses)
+    lane = lax.broadcasted_iota(jnp.int32, (1, 128), 1)
+    spread = sum(lse * (lane % heads == head).astype(jnp.float32) for head, lse in enumerate(lses))
+    total = jnp.zeros_like(spread)
+    for term in range(3):
+        rounded = spread.astype(jnp.bfloat16).astype(jnp.float32)
+        total = total + rounded * (lane // heads == term).astype(jnp.float32)
+        spread = spread - rounded
+    return total.astype(jnp.bfloat16)
+
+
+def band_bias(rows, width, offset, low, high):
+    query = lax.broadcasted_iota(jnp.int32, (rows, width), 0)
+    key = lax.broadcasted_iota(jnp.int32, (rows, width), 1)
+    step = key + offset - query
+    keep = (step >= -SIDE_STEPS) & (step <= SIDE_STEPS) & (key >= low) & (key < high)
+    return jnp.where(keep, 0.0, -1e30)
+
+
+def permutation(length, dilation, inverse):
+    row = lax.broadcasted_iota(jnp.int32, (length, length), 1 if inverse else 0)
+    column = lax.broadcasted_iota(jnp.int32, (length, length), 0 if inverse else 1)
+    steps = length // dilation
+    source = (row % steps) * dilation + row // steps
+    return (source == column).astype(jnp.float32).astype(jnp.bfloat16)
+
+
+def fused_kernel(
+    n, m, tokens_hbm, query_hbm, key_hbm, value_hbm, out_hbm, table_hbm, base_ref, result_ref,
+    tokens, weights, out_weight, table, kv_first, kv_middle, far_send, far_recv,
+    back_send, back_recv, merged_all, load_sem, weight_sem, local_sem,
+    near_send_sem, near_recv_sem, far_send_sem, far_recv_sem, back_send_sem, back_recv_sem,
+    tp_send_sem, tp_recv_sem,
+):
+    me = lax.axis_index("sp")
+    mine = lax.axis_index("tp")
+    length, columns = tokens.shape[0], weights.shape[-1]
+    half = HEAD_DIM // 2
+    classes = FAR_DILATION // n
+    halo = SIDE_STEPS
+
+    loads = [
+        pltpu.make_async_copy(tokens_hbm, tokens, load_sem.at[0]),
+        pltpu.make_async_copy(table_hbm, table, load_sem.at[1]),
+        pltpu.make_async_copy(out_hbm, out_weight, load_sem.at[2]),
+    ]
+    weight_loads = {}
+    loads[0].start()
+    for group in (2, 1, 0):
+        for kind, source in ((1, key_hbm), (2, value_hbm), (0, query_hbm)):
+            slot = group * 3 + kind
+            weight_loads[group, kind] = pltpu.make_async_copy(
+                source.at[group], weights.at[slot], weight_sem.at[slot]
+            )
+            weight_loads[group, kind].start()
+            if group == 2 and kind == 1:
+                loads[1].start()
+    loads[2].start()
+
+    barrier = pltpu.get_barrier_semaphore()
+    for distance in range(1, n):
+        pl.semaphore_signal(
+            barrier, inc=1, device_id={"sp": lax.rem(me + distance, n)}, device_id_type=MESH
+        )
+    for distance in range(1, m):
+        pl.semaphore_signal(
+            barrier, inc=1, device_id={"tp": lax.rem(mine + distance, m)}, device_id_type=MESH
+        )
+
+    @pl.when(me == 0)
+    def _():
+        kv_first[:, :halo] = jnp.zeros((2, halo, columns), jnp.bfloat16)
+        kv_middle[:, :, 0] = jnp.zeros_like(kv_middle[:, :, 0])
+
+    @pl.when(me == n - 1)
+    def _():
+        kv_first[:, halo + length :] = jnp.zeros((2, halo, columns), jnp.bfloat16)
+        kv_middle[:, :, 2] = jnp.zeros_like(kv_middle[:, :, 2])
+
+    loads[1].wait()
+    base_cos = base_ref[0, pl.ds(me, 1), :]
+    base_sin = base_ref[1, pl.ds(me, 1), :]
+    cosine = base_cos * table[0] - base_sin * table[1]
+    sine = base_sin * table[0] + base_cos * table[1]
+    wide = columns // cosine.shape[1]
+    lane = lax.broadcasted_iota(jnp.int32, (1, columns), 1)
+    first_half = lane % HEAD_DIM < half
+    cosine = jnp.concatenate([cosine] * wide, axis=1)
+    sine = jnp.concatenate([sine] * wide, axis=1) * jnp.where(first_half, -1.0, 1.0)
+    far_order = permutation(length, FAR_DILATION, False)
+    middle_order = permutation(length, MIDDLE_DILATION, False)
+    loads[0].wait()
+
+    def project(group, kind):
+        weight_loads[group, kind].wait()
+        product = jnp.dot(
+            tokens[...], weights[group * 3 + kind], preferred_element_type=jnp.float32
+        )
+        if kind < 2:
+            later = pltpu.roll(product, columns - half, 1)
+            earlier = pltpu.roll(product, half, 1)
+            product = product * cosine + jnp.where(first_half, later, earlier) * sine
+        if kind == 0:
+            product = product * HEAD_DIM ** (-0.5)
+        return product.astype(jnp.bfloat16)
+
+    def ordered(order, block):
+        return jnp.dot(order, block, preferred_element_type=jnp.float32).astype(jnp.bfloat16)
+
+    for kind in (1, 2, 0):
+        far_send[kind] = ordered(far_order, project(2, kind)).reshape(far_send.shape[1:])
+    pl.semaphore_wait(barrier, n - 1 + m - 1)
+    far_copies = []
+    for distance in range(1, n):
+        target = lax.rem(me + distance, n)
+        copy = remote(
+            far_send.at[:, pl.ds(target * classes, classes)],
+            far_recv.at[:, :, me],
+            far_send_sem.at[distance],
+            far_recv_sem.at[distance],
+            "sp",
+            target,
+        )
+        copy.start()
+        far_copies.append(copy)
+    far_own = pltpu.make_async_copy(
+        far_send.at[:, pl.ds(me * classes, classes)], far_recv.at[:, :, me], local_sem.at[0]
+    )
+    far_own.start()
+
+    for kind in (1, 2):
+        kv_middle[kind - 1, :, 1] = ordered(middle_order, project(1, kind)).reshape(
+            MIDDLE_DILATION, length // MIDDLE_DILATION, columns
+        )
+    middle_up = remote(
+        kv_middle.at[:, :, 1], kv_middle.at[:, :, 0],
+        near_send_sem.at[0], near_recv_sem.at[0], "sp", lax.rem(me + 1, n),
+    )
+    middle_down = remote(
+        kv_middle.at[:, :, 1], kv_middle.at[:, :, 2],
+        near_send_sem.at[1], near_recv_sem.at[1], "sp", lax.rem(me + n - 1, n),
+    )
+    first_up = remote(
+        kv_first.at[:, pl.ds(length, halo)], kv_first.at[:, pl.ds(0, halo)],
+        near_send_sem.at[2], near_recv_sem.at[2], "sp", lax.rem(me + 1, n),
+    )
+    first_down = remote(
+        kv_first.at[:, pl.ds(halo, halo)], kv_first.at[:, pl.ds(halo + length, halo)],
+        near_send_sem.at[3], near_recv_sem.at[3], "sp", lax.rem(me + n - 1, n),
+    )
+
+    @pl.when(me < n - 1)
+    def _():
+        middle_up.start()
+
+    @pl.when(me > 0)
+    def _():
+        middle_down.start()
+
+    for kind in (1, 2):
+        kv_first[kind - 1, halo : halo + length] = project(0, kind)
+
+    @pl.when(me < n - 1)
+    def _():
+        first_up.start()
+
+    @pl.when(me > 0)
+    def _():
+        first_down.start()
+
+    middle_queries = ordered(middle_order, project(1, 0))
+    first_queries = project(0, 0)
+
+    far_own.wait()
+    for copy in far_copies:
+        copy.wait()
+    class_len = n * (length // FAR_DILATION)
+    far_bias = band_bias(class_len, class_len, 0, 0, class_len)
+    for index in range(classes):
+        queries, keys, values = (
+            far_recv[kind, index].reshape(class_len, columns) for kind in range(3)
+        )
+        out, lses = attend(queries, keys, values, far_bias)
+        back_send[index, :, :, :columns] = out.astype(jnp.bfloat16).reshape(n, -1, columns)
+        back_send[index, :, :, columns:] = packed_lse(lses).reshape(n, -1, 128)
+    back_copies = []
+    for distance in range(1, n):
+        target = lax.rem(me + distance, n)
+        copy = remote(
+            back_send.at[:, target],
+            back_recv.at[pl.ds(me * classes, classes)],
+            back_send_sem.at[distance],
+            back_recv_sem.at[distance],
+            "sp",
+            target,
+        )
+        copy.start()
+        back_copies.append(copy)
+    back_own = pltpu.make_async_copy(
+        back_send.at[:, me], back_recv.at[pl.ds(me * classes, classes)], local_sem.at[1]
+    )
+    back_own.start()
+
+    @pl.when(me < n - 1)
+    def _():
+        first_up.wait_send()
+        first_down.wait_recv()
+
+    @pl.when(me > 0)
+    def _():
+        first_down.wait_send()
+        first_up.wait_recv()
+
+    tile = 2 * halo
+    first_outs = []
+    first_lses = []
+    for start in range(0, length, tile):
+        width = tile + 2 * halo
+        low = halo - start - me * length
+        high = halo - start + (n - me) * length
+        out, lses = attend(
+            first_queries[start : start + tile],
+            kv_first[0, start : start + width],
+            kv_first[1, start : start + width],
+            band_bias(tile, width, -halo, low, high),
+        )
+        first_outs.append(out)
+        first_lses.append(
+            sum(lse * head_mask(columns, head) for head, lse in enumerate(lses))
+        )
+    first_out = jnp.concatenate(first_outs, axis=0)
+    first_lse = jnp.concatenate(first_lses, axis=0)
+
+    @pl.when(me < n - 1)
+    def _():
+        middle_up.wait_send()
+        middle_down.wait_recv()
+
+    @pl.when(me > 0)
+    def _():
+        middle_down.wait_send()
+        middle_up.wait_recv()
+
+    steps = length // MIDDLE_DILATION
+    low = jnp.where(me == 0, steps, 0)
+    high = jnp.where(me == n - 1, 2 * steps, 3 * steps)
+    middle_bias = band_bias(steps, 3 * steps, -steps, low, high)
+    middle_parts = []
+    for index in range(MIDDLE_DILATION):
+        out, lses = attend(
+            middle_queries[index * steps : (index + 1) * steps],
+            kv_middle[0, index].reshape(3 * steps, columns),
+            kv_middle[1, index].reshape(3 * steps, columns),
+            middle_bias,
+        )
+        middle_parts.append(
+            jnp.concatenate([out.astype(jnp.bfloat16), packed_lse(lses)], axis=1)
+        )
+
+    heads = columns // HEAD_DIM
+    term = lax.broadcasted_iota(jnp.int32, (128, columns), 0)
+    column = lax.broadcasted_iota(jnp.int32, (128, columns), 1)
+    spread = (term % heads == column // HEAD_DIM) & (term < 3 * heads)
+    spread = spread.astype(jnp.float32).astype(jnp.bfloat16)
+
+    def natural(dilation, block):
+        block = jnp.dot(
+            permutation(length, dilation, True), block, preferred_element_type=jnp.float32
+        )
+        lse = jnp.dot(
+            block[:, columns:].astype(jnp.bfloat16), spread, preferred_element_type=jnp.float32
+        )
+        return block[:, :columns], lse
+
+    middle_out, middle_lse = natural(MIDDLE_DILATION, jnp.concatenate(middle_parts, axis=0))
+
+    back_own.wait()
+    for copy in back_copies:
+        copy.wait()
+    far_out, far_lse = natural(
+        FAR_DILATION, back_recv[...].reshape(length, back_recv.shape[2])
+    )
+
+    top = jnp.maximum(jnp.maximum(first_lse, middle_lse), far_lse)
+    first_w = jnp.exp(first_lse - top)
+    middle_w = jnp.exp(middle_lse - top)
+    far_w = jnp.exp(far_lse - top)
+    merged = (first_w * first_out + middle_w * middle_out + far_w * far_out) / (
+        first_w + middle_w + far_w
+    )
+    merged_all[0] = merged.astype(jnp.bfloat16)
+
+    tp_copies = []
+    for distance in range(1, m):
+        copy = remote(
+            merged_all.at[0],
+            merged_all.at[distance],
+            tp_send_sem.at[distance],
+            tp_recv_sem.at[distance],
+            "tp",
+            lax.rem(mine + distance, m),
+        )
+        copy.start()
+        tp_copies.append(copy)
+    loads[2].wait()
+    total = jnp.zeros(result_ref.shape, jnp.float32)
+    for distance in range(m):
+        if distance > 0:
+            tp_copies[distance - 1].wait()
+        owner = lax.rem(mine - distance + m, m)
+        rows = pl.ds(pl.multiple_of(owner * columns, columns), columns)
+        total = total + jnp.dot(
+            merged_all[distance], out_weight[rows, :], preferred_element_type=jnp.float32
+        )
+    result_ref[...] = total.astype(jnp.bfloat16)
+
+
+def turn_tables(n, length):
+    half = HEAD_DIM // 2
+    inverse = 1.0 / 10000.0 ** (np.arange(half, dtype=np.float32) * np.float32(2.0) / HEAD_DIM)
+    inverse = np.tile(inverse.astype(np.float64), 128 // half)[None]
+    inner = np.arange(length)[:, None] * inverse
+    outer = (np.arange(n) * length)[:, None] * inverse
+    table = np.stack([np.cos(inner), np.sin(inner)]).astype(np.float32)
+    base = np.stack([np.cos(outer), np.sin(outer)]).astype(np.float32)
+    return table, base
+
+
+def fused(n, m, tokens, query_weight, key_weight, value_weight, out_weight):
+    length, width = tokens.shape
+    columns = query_weight.shape[2]
+    table, base = turn_tables(n, length)
+    steps = length // FAR_DILATION
+    classes = FAR_DILATION // n
+    kept = columns + 128
+    bf16 = jnp.bfloat16
+    hbm = pl.BlockSpec(memory_space=pl.ANY)
+    vmem = pl.BlockSpec(memory_space=pltpu.VMEM)
+    dma = pltpu.SemaphoreType.DMA
+    return pl.pallas_call(
+        functools.partial(fused_kernel, n, m),
+        out_shape=jax.ShapeDtypeStruct((length, out_weight.shape[1]), bf16),
+        in_specs=[hbm] * 6 + [vmem],
+        out_specs=vmem,
+        scratch_shapes=[
+            pltpu.VMEM((length, width), bf16),
+            pltpu.VMEM((9, width, columns), bf16),
+            pltpu.VMEM(out_weight.shape, bf16),
+            pltpu.VMEM(table.shape, jnp.float32),
+            pltpu.VMEM((2, length + 2 * SIDE_STEPS, columns), bf16),
+            pltpu.VMEM((2, MIDDLE_DILATION, 3, length // MIDDLE_DILATION, columns), bf16),
+            pltpu.VMEM((3, FAR_DILATION, steps, columns), bf16),
+            pltpu.VMEM((3, classes, n, steps, columns), bf16),
+            pltpu.VMEM((classes, n, steps, kept), bf16),
+            pltpu.VMEM((FAR_DILATION, steps, kept), bf16),
+            pltpu.VMEM((m, length, columns), bf16),
+            dma((3,)),
+            dma((9,)),
+            dma((2,)),
+            dma((4,)),
+            dma((4,)),
+            dma((n,)),
+            dma((n,)),
+            dma((n,)),
+            dma((n,)),
+            dma((m,)),
+            dma((m,)),
+        ],
+        compiler_params=pltpu.CompilerParams(
+            collective_id=0, has_side_effects=True, vmem_limit_bytes=60 * 1024 * 1024
+        ),
+    )(tokens, query_weight, key_weight, value_weight, out_weight, jnp.asarray(table), jnp.asarray(base))
+
+
+def planned(n, m, *arrays):
+    length, columns = arrays[0].shape[0], arrays[1].shape[2]
+    fits = (
+        n > 1
+        and m > 1
+        and FAR_DILATION % n == 0
+        and length == SIDE_STEPS * MIDDLE_DILATION
+        and length % (FAR_DILATION * 16) == 0
+        and columns % 128 == 0
+        and 3 * (columns // HEAD_DIM) <= 128
+    )
+    if fits:
+        return fused(n, m, *arrays)
+    return per_device(*arrays)
+
+
 def solution(mesh):
     placed = (
         P("sp", None),
@@ -166,5 +599,9 @@
         P(None, "tp"),
     )
     return jax.shard_map(
-        per_device, mesh=mesh, in_specs=placed, out_specs=P("sp", "tp"), check_vma=False
-    )
+        functools.partial(planned, mesh.shape["sp"], mesh.shape["tp"]),
+        mesh=mesh,
+        in_specs=placed,
+        out_specs=P("sp", "tp"),
+        check_vma=False,
+    )

time: 189 us -> 42.4 us (0.22); the launches traced: 186 us -> 41.8 us
  local copies, waits for them, and re-layouts: 93.4 us -> 1.67 us
  Pallas kernels: 0 us -> 40.1 us
  starting transfers between devices: 30.1 us -> 0 us
  matrix products: 26.3 us -> 0 us
  other arithmetic: 20.8 us -> 0 us
  blocking collectives: 9.17 us -> 0 us
  waiting for transfers between devices: 4.95 us -> 0 us
    slice x58 -> x0, local copies, waits for them, and re-layouts: 46.9 us -> none  [the longest x32 29.6 us: banded(): value_blocks[shift_idx:shift_idx + blocks]]
    pallas_call x0 -> x1, Pallas kernels: none -> 40.1 us  [fused(): pl.pallas_call(functools.partial(fused_kernel, n, m), out_shape=jax.Shape...]
    ppermute x10 -> x0, starting transfers between devices: 30.1 us -> none  [the longest x6 18.2 us: shifted(): return lax.ppermute(block, axis, route)]
    dot_general x16 -> x0, matrix products: 26.3 us -> none  [the longest x3 6.48 us: per_device(): jnp.dot(tokens, query_weight[group_idx], preferred_element_type=jnp.float32)]
    concatenate x2 -> x0, local copies, waits for them, and re-layouts: 19.9 us -> none  [the longest x1 10.3 us: banded(): jnp.concatenate([value_blocks[shift_idx:shift_idx + blocks] for shift_idx...]
    dot_general x8 -> x0, local copies, waits for them, and re-layouts: 15.1 us -> none  [the longest x4 7.65 us: per_device(): jnp.dot(tokens, query_weight[group_idx], preferred_element_type=jnp.float32)]
    all_gather x1 -> x0, blocking collectives: 9.17 us -> none  [per_device(): lax.all_gather(merged, 'tp', axis=1, tiled=True)]
    and x7 -> x0, other arithmetic: 5.2 us -> none  [the longest x4 3.86 us: banded(): within[None, None, None]]
  transfers between devices with their start and end apart: 10 -> 0, of which waited for: 2 -> 0; matrix products, arithmetic and copies ran while one was open for 34% -> 0% of each run, Pallas kernels for 0% -> 0%
where the time goes in v1:
time: 42.4 us; the launch traced here: 41.8 us
  Pallas kernels  40.1 us (95%)
  local copies, waits for them, and re-layouts  1.67 us (4%)
    pallas_call x1, Pallas kernels, fused(): pl.pallas_call(functools.partial(fused_kernel, n, m), out_shape=jax.Shape...  40.1 us
    unnamed x1, local copies, waits for them, and re-layouts  1.67 us

profile of v1, /device:TPU:9, one launch (start us, length us, event | category | flops | bytes accessed | tf_op | source)
XLA Modules:
  0.0 41.8 jit_solution(8988347262220111498)
XLA Ops:
  0.0 40.1 %shard_map.73 = bf16[256,512]{1,0:T(8,128)(2,1)} custom-call(bf16[256,2048]{1,0:T(8,128)(2,1)} %tokens_hbm.1, bf16[3,2048,256]{2,1,0:T(8,128)(2,1)} %query_hbm.1, bf16[3,2048,256]{2,1,0:T(8,128)(2,1)} %key_hbm.1, bf16[3,2048,256]{2,1,0:T(8,128)(2,1)} %value_hbm.1, bf16[1024,512]{1,0:T(8,128)(2,1)} %out_hbm.1, f32[2,256,128]{2,1,0:T(8,128)} %constant.4.clone.table_hbm, ...), custom_call_target="tpu_custom_call" | custom-call | tf_op jit(solution)/shard_map/pallas_call | solution.py:542
  40.1 1.7 %copy.9 = bf16[256,512]{1,0:T(8,128)(2,1)} copy(bf16[256,512]{1,0:T(8,128)(2,1)} %shard_map.73) | data formatting | bytes 524288

commit v2 on v1

--- a/solution.py
+++ b/solution.py
@@ -247,17 +247,18 @@
         pltpu.make_async_copy(out_hbm, out_weight, load_sem.at[2]),
     ]
     weight_loads = {}
-    loads[0].start()
     for group in (2, 1, 0):
         for kind, source in ((1, key_hbm), (2, value_hbm), (0, query_hbm)):
             slot = group * 3 + kind
             weight_loads[group, kind] = pltpu.make_async_copy(
                 source.at[group], weights.at[slot], weight_sem.at[slot]
             )
-            weight_loads[group, kind].start()
-            if group == 2 and kind == 1:
-                loads[1].start()
-    loads[2].start()
+    loads[0].start()
+    loads[1].start()
+    for kind in (1, 2, 0):
+        weight_loads[2, kind].start()
+    later_loads = [weight_loads[group, kind] for group in (1, 0) for kind in (1, 2)]
+    later_loads += [weight_loads[1, 0], weight_loads[0, 0], loads[2]]
 
     barrier = pltpu.get_barrier_semaphore()
     for distance in range(1, n):
@@ -309,22 +310,26 @@
     def ordered(order, block):
         return jnp.dot(order, block, preferred_element_type=jnp.float32).astype(jnp.bfloat16)
 
+    far_copies = []
     for kind in (1, 2, 0):
         far_send[kind] = ordered(far_order, project(2, kind)).reshape(far_send.shape[1:])
-    pl.semaphore_wait(barrier, n - 1 + m - 1)
-    far_copies = []
-    for distance in range(1, n):
-        target = lax.rem(me + distance, n)
-        copy = remote(
-            far_send.at[:, pl.ds(target * classes, classes)],
-            far_recv.at[:, :, me],
-            far_send_sem.at[distance],
-            far_recv_sem.at[distance],
-            "sp",
-            target,
-        )
-        copy.start()
-        far_copies.append(copy)
+        for load in later_loads[:3]:
+            load.start()
+        later_loads = later_loads[3:]
+        if kind == 1:
+            pl.semaphore_wait(barrier, n - 1 + m - 1)
+        for distance in range(1, n):
+            target = lax.rem(me + distance, n)
+            copy = remote(
+                far_send.at[kind, pl.ds(target * classes, classes)],
+                far_recv.at[kind, :, me],
+                far_send_sem.at[kind, distance],
+                far_recv_sem.at[kind, distance],
+                "sp",
+                target,
+            )
+            copy.start()
+            far_copies.append(copy)
     far_own = pltpu.make_async_copy(
         far_send.at[:, pl.ds(me * classes, classes)], far_recv.at[:, :, me], local_sem.at[0]
     )
@@ -492,29 +497,55 @@
     )
     merged_all[0] = merged.astype(jnp.bfloat16)
 
-    tp_copies = []
-    for distance in range(1, m):
+    chips = m // 2
+    sibling = mine + 1 - 2 * lax.rem(mine, 2)
+    piece = length // 2
+
+    def hand(part, source, slot, target):
+        rows = pl.ds(part * piece, piece)
         copy = remote(
-            merged_all.at[0],
-            merged_all.at[distance],
-            tp_send_sem.at[distance],
-            tp_recv_sem.at[distance],
+            merged_all.at[source, rows],
+            merged_all.at[slot, rows],
+            tp_send_sem.at[part, slot],
+            tp_recv_sem.at[part, slot],
             "tp",
-            lax.rem(mine + distance, m),
+            target,
         )
         copy.start()
-        tp_copies.append(copy)
+        return copy
+
+    copies = {}
+    for part in range(2):
+        for chip in range(1, chips):
+            copies[part, chip] = hand(part, 0, chip, lax.rem(mine + 2 * chip, m))
+    for part in range(2):
+        copies[part, chips] = hand(part, 0, chips, sibling)
     loads[2].wait()
-    total = jnp.zeros(result_ref.shape, jnp.float32)
-    for distance in range(m):
-        if distance > 0:
-            tp_copies[distance - 1].wait()
-        owner = lax.rem(mine - distance + m, m)
+
+    def term(part, slot):
+        chip = slot % chips
+        owner = lax.rem((mine if slot < chips else sibling) - 2 * chip + m, m)
         rows = pl.ds(pl.multiple_of(owner * columns, columns), columns)
-        total = total + jnp.dot(
-            merged_all[distance], out_weight[rows, :], preferred_element_type=jnp.float32
-        )
-    result_ref[...] = total.astype(jnp.bfloat16)
+        return jnp.dot(
+            merged_all[slot, part * piece : (part + 1) * piece],
+            out_weight[rows, :],
+            preferred_element_type=jnp.float32,
+        )
+
+    totals = [term(part, 0) for part in range(2)]
+    for part in range(2):
+        for chip in range(1, chips):
+            copies[part, chip].wait()
+            copies[part, chips + chip] = hand(part, chip, chips + chip, sibling)
+        copies[part, chips].wait()
+        totals[part] = totals[part] + term(part, chips)
+        for chip in range(1, chips):
+            totals[part] = totals[part] + term(part, chip)
+    for part in range(2):
+        for chip in range(1, chips):
+            copies[part, chips + chip].wait()
+            totals[part] = totals[part] + term(part, chips + chip)
+        result_ref[part * piece : (part + 1) * piece] = totals[part].astype(result_ref.dtype)
 
 
 def turn_tables(n, length):
@@ -541,7 +572,7 @@
     dma = pltpu.SemaphoreType.DMA
     return pl.pallas_call(
         functools.partial(fused_kernel, n, m),
-        out_shape=jax.ShapeDtypeStruct((length, out_weight.shape[1]), bf16),
+        out_shape=jax.ShapeDtypeStruct((length, out_weight.shape[1]), jnp.float32),
         in_specs=[hbm] * 6 + [vmem],
         out_specs=vmem,
         scratch_shapes=[
@@ -561,24 +592,24 @@
             dma((2,)),
             dma((4,)),
             dma((4,)),
+            dma((3, n)),
+            dma((3, n)),
             dma((n,)),
             dma((n,)),
-            dma((n,)),
-            dma((n,)),
-            dma((m,)),
-            dma((m,)),
+            dma((2, m)),
+            dma((2, m)),
         ],
         compiler_params=pltpu.CompilerParams(
             collective_id=0, has_side_effects=True, vmem_limit_bytes=60 * 1024 * 1024
         ),
-    )(tokens, query_weight, key_weight, value_weight, out_weight, jnp.asarray(table), jnp.asarray(base))
+    )(tokens, query_weight, key_weight, value_weight, out_weight, jnp.asarray(table), jnp.asarray(base)).astype(bf16)
 
 
 def planned(n, m, *arrays):
     length, columns = arrays[0].shape[0], arrays[1].shape[2]
     fits = (
         n > 1
-        and m > 1
+        and m % 2 == 0
         and FAR_DILATION % n == 0
         and length == SIDE_STEPS * MIDDLE_DILATION
         and length % (FAR_DILATION * 16) == 0

time: 42.4 us -> 39.9 us (0.941)
  Pallas kernels: 40.1 us -> 37.5 us
  other arithmetic: 0 us -> 1.78 us
  local copies, waits for them, and re-layouts: 1.67 us -> 0 us
    pallas_call x1, Pallas kernels: 40.1 us -> 37.5 us  [fused(): pl.pallas_call(functools.partial(fused_kernel, n, m), out_shape=jax.Shape...]
    convert_element_type x0 -> x1, other arithmetic: none -> 1.78 us  [fused(): return pl.pallas_call(functools.partial(fused_kernel, n, m), out_shape=ja...]
    unnamed x1 -> x0, local copies, waits for them, and re-layouts: 1.67 us -> none
where the time goes in v2:
time: 39.9 us; the launch traced here: 39.3 us
  Pallas kernels  37.5 us (94%)
  other arithmetic  1.78 us (4%)
    pallas_call x1, Pallas kernels, fused(): pl.pallas_call(functools.partial(fused_kernel, n, m), out_shape=jax.Shape...  37.5 us
    convert_element_type x1, other arithmetic, fused(): return pl.pallas_call(functools.partial(fused_kernel, n, m), out_shape=ja...  1.78 us

profile of v2, /device:TPU:9, one launch (start us, length us, event | category | flops | bytes accessed | tf_op | source)
XLA Modules:
  0.0 39.3 jit_solution(1718550336692124714)
XLA Ops:
  0.0 37.5 %shard_map.73 = f32[256,512]{1,0:T(8,128)} custom-call(bf16[256,2048]{1,0:T(8,128)(2,1)} %tokens_hbm.1, bf16[3,2048,256]{2,1,0:T(8,128)(2,1)} %query_hbm.1, bf16[3,2048,256]{2,1,0:T(8,128)(2,1)} %key_hbm.1, bf16[3,2048,256]{2,1,0:T(8,128)(2,1)} %value_hbm.1, bf16[1024,512]{1,0:T(8,128)(2,1)} %out_hbm.1, f32[2,256,128]{2,1,0:T(8,128)} %constant.4.clone.table_hbm, ...), custom_call_target="tpu_custom_call" | custom-call | tf_op jit(solution)/shard_map/pallas_call | solution.py:573
  37.5 1.8 %convert_element_type.3 = bf16[256,512]{1,0:T(8,128)(2,1)} convert(f32[256,512]{1,0:T(8,128)} %shard_map.73) | non-fusion elementwise | flops 131072 | bytes 786432 | tf_op jit(solution)/shard_map/convert_element_type | solution.py:605

commit v3 on v2

--- a/solution.py
+++ b/solution.py
@@ -257,7 +257,7 @@
     loads[1].start()
     for kind in (1, 2, 0):
         weight_loads[2, kind].start()
-    later_loads = [weight_loads[group, kind] for group in (1, 0) for kind in (1, 2)]
+    later_loads = [weight_loads[group, kind] for group in (0, 1) for kind in (1, 2)]
     later_loads += [weight_loads[1, 0], weight_loads[0, 0], loads[2]]
 
     barrier = pltpu.get_barrier_semaphore()
@@ -335,27 +335,38 @@
     )
     far_own.start()
 
+    middle_up = remote(
+        kv_middle.at[:, :, 1], kv_middle.at[:, :, 0],
+        near_send_sem.at[0], near_recv_sem.at[0], "sp", lax.rem(me + 1, n),
+    )
+    middle_down = remote(
+        kv_middle.at[:, :, 1], kv_middle.at[:, :, 2],
+        near_send_sem.at[1], near_recv_sem.at[1], "sp", lax.rem(me + n - 1, n),
+    )
+    first_up = remote(
+        kv_first.at[:, pl.ds(length, halo)], kv_first.at[:, pl.ds(0, halo)],
+        near_send_sem.at[2], near_recv_sem.at[2], "sp", lax.rem(me + 1, n),
+    )
+    first_down = remote(
+        kv_first.at[:, pl.ds(halo, halo)], kv_first.at[:, pl.ds(halo + length, halo)],
+        near_send_sem.at[3], near_recv_sem.at[3], "sp", lax.rem(me + n - 1, n),
+    )
+
+    for kind in (1, 2):
+        kv_first[kind - 1, halo : halo + length] = project(0, kind)
+
+    @pl.when(me < n - 1)
+    def _():
+        first_up.start()
+
+    @pl.when(me > 0)
+    def _():
+        first_down.start()
+
     for kind in (1, 2):
         kv_middle[kind - 1, :, 1] = ordered(middle_order, project(1, kind)).reshape(
             MIDDLE_DILATION, length // MIDDLE_DILATION, columns
         )
-    middle_up = remote(
-        kv_middle.at[:, :, 1], kv_middle.at[:, :, 0],
-        near_send_sem.at[0], near_recv_sem.at[0], "sp", lax.rem(me + 1, n),
-    )
-    middle_down = remote(
-        kv_middle.at[:, :, 1], kv_middle.at[:, :, 2],
-        near_send_sem.at[1], near_recv_sem.at[1], "sp", lax.rem(me + n - 1, n),
-    )
-    first_up = remote(
-        kv_first.at[:, pl.ds(length, halo)], kv_first.at[:, pl.ds(0, halo)],
-        near_send_sem.at[2], near_recv_sem.at[2], "sp", lax.rem(me + 1, n),
-    )
-    first_down = remote(
-        kv_first.at[:, pl.ds(halo, halo)], kv_first.at[:, pl.ds(halo + length, halo)],
-        near_send_sem.at[3], near_recv_sem.at[3], "sp", lax.rem(me + n - 1, n),
-    )
-
     @pl.when(me < n - 1)
     def _():
         middle_up.start()
@@ -363,17 +374,6 @@
     @pl.when(me > 0)
     def _():
         middle_down.start()
-
-    for kind in (1, 2):
-        kv_first[kind - 1, halo : halo + length] = project(0, kind)
-
-    @pl.when(me < n - 1)
-    def _():
-        first_up.start()
-
-    @pl.when(me > 0)
-    def _():
-        first_down.start()
 
     middle_queries = ordered(middle_order, project(1, 0))
     first_queries = project(0, 0)

time: 39.9 us -> 39 us (0.977); the launches traced: 39.3 us -> 38.8 us
  Pallas kernels: 37.5 us -> 37 us
    pallas_call x1, Pallas kernels: 37.5 us -> 37 us  [fused(): pl.pallas_call(functools.partial(fused_kernel, n, m), out_shape=jax.Shape...]
where the time goes in v3:
time: 39 us; the launch traced here: 38.8 us
  Pallas kernels  37 us (95%)
  other arithmetic  1.78 us (5%)
    pallas_call x1, Pallas kernels, fused(): pl.pallas_call(functools.partial(fused_kernel, n, m), out_shape=jax.Shape...  37 us
    convert_element_type x1, other arithmetic, fused(): return pl.pallas_call(functools.partial(fused_kernel, n, m), out_shape=ja...  1.78 us

profile of v3, /device:TPU:9, one launch (start us, length us, event | category | flops | bytes accessed | tf_op | source)
XLA Modules:
  0.0 38.8 jit_solution(15062129707214325516)
XLA Ops:
  0.0 37.0 %shard_map.73 = f32[256,512]{1,0:T(8,128)} custom-call(bf16[256,2048]{1,0:T(8,128)(2,1)} %tokens_hbm.1, bf16[3,2048,256]{2,1,0:T(8,128)(2,1)} %query_hbm.1, bf16[3,2048,256]{2,1,0:T(8,128)(2,1)} %key_hbm.1, bf16[3,2048,256]{2,1,0:T(8,128)(2,1)} %value_hbm.1, bf16[1024,512]{1,0:T(8,128)(2,1)} %out_hbm.1, f32[2,256,128]{2,1,0:T(8,128)} %constant.4.clone.table_hbm, ...), custom_call_target="tpu_custom_call" | custom-call | tf_op jit(solution)/shard_map/pallas_call | solution.py:573
  37.0 1.8 %convert_element_type.3 = bf16[256,512]{1,0:T(8,128)(2,1)} convert(f32[256,512]{1,0:T(8,128)} %shard_map.73) | non-fusion elementwise | flops 131072 | bytes 786432 | tf_op jit(solution)/shard_map/convert_element_type | solution.py:605
